TPU v7x, 32 devices: a whole 2x2x4 slice. The times are simulated.
32 devices in a mesh: sp: 4 (over y, x), tp: 8 (over z, core).
Axes of the slice: x: 2, y: 2, z: 4, core: 2. Of those that a mesh axis runs over, the one named last changes fastest.
Arguments:
- queries: bfloat16 [1536, 2048], P('sp', 'tp'), may hold values from -6 to 6
- keys: bfloat16 [1536, 2048], P('sp', 'tp'), may hold values from -6 to 6
- values: bfloat16 [1536, 2048], P('sp', 'tp'), may hold values from -6 to 6
- key_bias: bfloat16 [1536, 32], P('sp', 'tp'), may hold values from -16 to 0
- head_gain: float32 [32, 64], P('tp'), may hold values from 0.1 to 1.9
- out_weight: bfloat16 [2048, 2048], P('tp'), may hold values from -0.125 to 0.125
- residual: bfloat16 [1536, 2048], P(('sp', 'tp')), may hold values from -6 to 6
- norm_gain: float32 [2048], replicated, may hold values from 0.1 to 1.9
- gate_proj: bfloat16 [4, 2048, 7168], P('sp', None, 'tp'), may hold values from -0.125 to 0.125
- up_proj: bfloat16 [4, 2048, 7168], P('sp', None, 'tp'), may hold values from -0.125 to 0.125
- down_proj: bfloat16 [4, 7168, 2048], P('sp', 'tp'), may hold values from -0.0625 to 0.0625
- expert_choice: int32 [1536, 2], P(('sp', 'tp')), may hold values from 0 to 3, all different within a row; in each aligned block of 48 rows (0 to 47, 48 to 95, ...) at most 48 rows name the same one
- expert_weights: float32 [1536, 2], P(('sp', 'tp')), may hold values from 0.2 to 1
Outputs:
- layer_out: bfloat16 [1536, 2048], P(('sp', 'tp'))
Inputs may be any that keep to these rules, and one draw needn't show every extreme that they name: `expert_choice`: in each aligned block of 48 rows (the rows of one device), no expert is named more than 48 times; the two experts of a row differ.
All inputs are finite; a program needn't handle non-finite values.
Results may differ from a plain program's by a relative error of at most 0.019.
Values may be sent and summed in bfloat16 or wider, within the bound.
A program may use at most 128 MiB of HBM per device.

v0:
```python
import jax
import jax.numpy as jnp
from jax import lax
from jax.sharding import PartitionSpec as P

epsilon = 1e-06


def rms_scaled(values_in):
    return values_in * lax.rsqrt(jnp.mean(values_in * values_in, axis=-1, keepdims=True) + epsilon)


def expert_partial(row_block, gate_matrix, up_matrix, down_matrix):
    gate_part = jnp.dot(row_block, gate_matrix, preferred_element_type=jnp.float32)
    up_part = jnp.dot(row_block, up_matrix, preferred_element_type=jnp.float32)
    hidden = (jax.nn.silu(gate_part) * up_part).astype(jnp.bfloat16)
    return jnp.dot(hidden, down_matrix, preferred_element_type=jnp.float32)


def choice_ranks(routes, experts_all):
    flat_routes = routes.reshape(routes.shape[:-2] + (-1,))
    onehot = (flat_routes[..., None] == jnp.arange(experts_all, dtype=jnp.int32)).astype(jnp.int32)
    before = jnp.cumsum(onehot, axis=-2) - onehot
    return jnp.sum(before * onehot, axis=-1).reshape(routes.shape)


def slot_tokens(slot_index, targets, missing):
    flat_slots = slot_index.reshape(-1)
    owners = jnp.arange(flat_slots.shape[0], dtype=jnp.int32) // 2
    matches = flat_slots[None, :] == jnp.arange(targets, dtype=jnp.int32)[:, None]
    owner_found = jnp.sum(jnp.where(matches, owners[None, :], 0), axis=1)
    return jnp.where(jnp.any(matches, axis=1), owner_found, missing)


def on_device(
    queries,
    keys,
    values,
    key_bias,
    head_gain,
    out_weight,
    residual,
    norm_gain,
    gate_proj,
    up_proj,
    down_proj,
    expert_choice,
    expert_weights,
):
    rows_own = queries.shape[0]
    heads_here = head_gain.shape[0]
    head_size = head_gain.shape[1]
    model_width = out_weight.shape[1]
    seq_devices = lax.axis_size("sp")
    head_devices = lax.axis_size("tp")
    own_start = lax.axis_index("sp") * rows_own
    query_pos = own_start + jnp.arange(rows_own, dtype=jnp.int32)
    query_heads = queries.reshape(rows_own, heads_here, head_size)

    def key_block(slot_state, key_rows, value_rows, bias_rows, key_start):
        key_heads = key_rows.reshape(rows_own, heads_here, head_size)
        value_heads = value_rows.reshape(rows_own, heads_here, head_size)
        scores = jnp.einsum(
            "qhd,khd->hqk", query_heads, key_heads, preferred_element_type=jnp.float32
        ) * head_size ** (-0.5)
        scores = scores + bias_rows.astype(jnp.float32).T[:, None, :]
        key_pos = key_start + jnp.arange(rows_own, dtype=jnp.int32)
        earlier = (key_pos[None, :] < query_pos[:, None])[None, :, :]
        log_drops = jnp.where(earlier, jax.nn.log_sigmoid(-scores), 0.0)
        suffix = lax.cumsum(log_drops, axis=2, reverse=True) - log_drops
        within = jnp.where(earlier, jnp.exp(jax.nn.log_sigmoid(scores) + suffix), 0.0).astype(
            jnp.bfloat16
        )
        block_part = jnp.einsum(
            "hqk,khd->qhd", within, value_heads, preferred_element_type=jnp.float32
        )
        block_index = key_start // rows_own
        sums_new = lax.dynamic_update_index_in_dim(
            slot_state[0], block_part.reshape(rows_own, heads_here * head_size), block_index, 0
        )
        totals_new = lax.dynamic_update_index_in_dim(
            slot_state[1], jnp.sum(log_drops, axis=2), block_index, 0
        )
        return (sums_new, totals_new)

    empty_state = (
        jnp.zeros((seq_devices, rows_own, heads_here * head_size), jnp.float32),
        jnp.zeros((seq_devices, heads_here, rows_own), jnp.float32),
    )
    key_piece = lax.all_gather(keys, "sp", axis=0, tiled=True)
    value_piece = lax.all_gather(values, "sp", axis=0, tiled=True)
    bias_piece = lax.all_gather(key_bias, "sp", axis=0, tiled=True)

    def visit(block_count, state_in):
        offset = block_count * rows_own

        def take_rows(array):
            return lax.dynamic_slice_in_dim(array, offset, rows_own, 0)

        def compute(state_now):
            return key_block(
                state_now,
                take_rows(key_piece),
                take_rows(value_piece),
                take_rows(bias_piece),
                offset,
            )

        def keep(state_now):
            return state_now

        return lax.cond(offset <= own_start, compute, keep, state_in)

    block_sums, totals = lax.fori_loop(0, key_piece.shape[0] // rows_own, visit, empty_state)
    carried = jnp.sum(totals, axis=0, keepdims=True) - jnp.cumsum(totals, axis=0)
    factors = jnp.exp(carried).transpose(0, 2, 1)[..., None]
    mixture = jnp.sum(
        factors * block_sums.reshape(seq_devices, rows_own, heads_here, head_size), axis=0
    )
    attended = (
        (rms_scaled(mixture) * head_gain)
        .astype(jnp.bfloat16)
        .reshape(rows_own, heads_here * head_size)
    )
    row_share = rows_own // head_devices
    merged = lax.all_to_all(attended, "tp", split_axis=0, concat_axis=1, tiled=True)
    projected = jnp.dot(
        merged,
        lax.all_gather(out_weight, "tp", axis=0, tiled=True),
        preferred_element_type=jnp.float32,
    )
    stream = (residual.astype(jnp.float32) + projected).astype(jnp.bfloat16)
    normed = (rms_scaled(stream.astype(jnp.float32)) * norm_gain).astype(jnp.bfloat16)
    local_experts = gate_proj.shape[0]
    experts_all = local_experts * seq_devices
    capacity = 4 * rows_own // (head_devices * experts_all)
    own_slots = expert_choice * capacity + choice_ranks(expert_choice, experts_all)
    wanted = slot_tokens(own_slots, experts_all * capacity, row_share)
    outgoing = jnp.take(normed, wanted, axis=0, mode="fill", fill_value=0)
    arrived = lax.all_to_all(
        outgoing.reshape(seq_devices, local_experts, capacity, model_width),
        "sp",
        split_axis=0,
        concat_axis=0,
        tiled=True,
    )
    row_piece = lax.all_gather(arrived, "tp", axis=0, tiled=True)
    count_rows = row_piece.shape[0]
    partials = jnp.stack(
        [
            expert_partial(
                row_piece[:, 0].reshape(-1, model_width), gate_proj[0], up_proj[0], down_proj[0]
            ).reshape(count_rows, capacity, model_width)
        ],
        axis=1,
    )
    summed = lax.psum_scatter(partials.astype(jnp.bfloat16), "tp", scatter_dimension=0, tiled=True)
    returned = lax.all_to_all(summed, "sp", split_axis=0, concat_axis=0, tiled=True).reshape(
        experts_all * capacity, model_width
    )
    picked = jnp.take(returned, own_slots, axis=0).astype(jnp.float32)
    combined = jnp.sum(expert_weights[:, :, None] * picked, axis=1)
    return (stream.astype(jnp.float32) + combined).astype(jnp.bfloat16)


def solution(mesh):
    placed = (
        P("sp", "tp"),
        P("sp", "tp"),
        P("sp", "tp"),
        P("sp", "tp"),
        P("tp", None),
        P("tp", None),
        P(("sp", "tp"), None),
        P(),
        P("sp", None, "tp"),
        P("sp", None, "tp"),
        P("sp", "tp", None),
        P(("sp", "tp"), None),
        P(("sp", "tp"), None),
    )
    return jax.shard_map(
        on_device, mesh=mesh, in_specs=placed, out_specs=P(("sp", "tp"), None), check_vma=False
    )
```

profile of v0, /device:TPU:0, one launch (start us, length us, event | category | flops | bytes accessed | tf_op | source)
XLA Modules:
  0.0 380.5 jit_solution(13210839301603181166)
XLA Ops:
  6.5 0.7 all-gather.3.cloned.1.call-update
  7.3 1.1 copy.81
  8.4 1.1 copy.82
  9.4 1.7 copy.83
  11.2 11.0 %all_gather.17 = bf16[1536,4]{0,1:T(4,128)(2,1)} all-gather(bf16[384,4]{0,1:T(4,128)(2,1)} %param.20), channel_id=1, replica_groups=mesh['sp'=4,'tp'=8] {'sp'}, dimensions={0}, use_global_device_ids=true | all-gather | bytes 15360 | tf_op jit(solution)/shard_map/all_gather | solution.py:92
  22.2 12.4 %all_gather.15 = bf16[1536,256]{0,1:T(8,128)(2,1)} all-gather(bf16[384,256]{0,1:T(8,128)(2,1)S(1)} %copy.81), channel_id=1, replica_groups=mesh['sp'=4,'tp'=8] {'sp'}, dimensions={0}, use_global_device_ids=true | all-gather | bytes 983040 | tf_op jit(solution)/shard_map/all_gather | solution.py:91
  34.5 13.4 %all_gather.16 = bf16[1536,256]{0,1:T(8,128)(2,1)} all-gather(bf16[384,256]{0,1:T(8,128)(2,1)S(1)} %copy.82), channel_id=1, replica_groups=mesh['sp'=4,'tp'=8] {'sp'}, dimensions={0}, use_global_device_ids=true | all-gather | bytes 983040 | tf_op jit(solution)/shard_map/all_gather | solution.py:90
  47.9 1.3 broadcast_in_dim.84
  49.2 0.6 broadcast_in_dim.85
  49.8 28.2 %while.17 = (s32[]{:T(128)}, f32[4,384,256]{1,2,0:T(8,128)}, f32[4,4,384]{2,1,0:T(4,128)}, s32[]{:T(128)}, bf16[1536,256]{0,1:T(8,128)(2,1)}, /*index=5*/bf16[15...) while((s32[]{:T(128)}, f32[4,384,256]{1,2,0:T(8,128)}, ...), condition=%wide.region_6.7_spmd.clone.clone, body=%wide.region_0.6_spmd.clone.clone.sunk | while | flops 246117120 | bytes 38572464 | solution.py:114
  49.8 28.0 %conditional.4 = ((f32[4,384,256]{1,2,0:T(8,128)}, f32[4,4,384]{2,1,0:T(4,128)})) conditional(s32[]{:T(128)} %convert_element_type.76, (f32[4,384,256]{1,2,0:T(8,128)}, f32[4,4,384]{2,1,0:T(4,128)}) %tuple.53, (s32[]{:T(128)}, bf16[1536,256]{0,1:T(8,128)(2,1)}, s32[]{:T(128)}, bf16[1536,256]{0,1:T(8,128)(2,1)}, bf16[384,4,64]{0,2,1:T(8,128)(2,1)}, ...), branch_computations={%region_1.0_spmd, %region_2.5_spmd} | conditional | flops 246117120 | bytes 38570716 | solution.py:112
  49.8 1.1 constant_dynamic-slice_fusion
  50.8 0.7 convert_bitcast_fusion
  51.5 0.1 broadcast_compare_fusion
  51.7 4.3 %fusion.15 = (f32[4,384]{1,0:T(4,128)S(1)}, f32[4,384,384]{1,2,0:T(8,128)S(1)}, f32[4,384,384]{2,1,0:T(8,128)}) fusion(f32[4,384]{1,0:T(4,128)S(1)} %convert_bitcast_fusion, pred[384,384]{0,1:T(8,128)(4,1)S(1)} %broadcast_compare_fusion, bf16[384,4,64]{0,2,1:T(8,128)(2,1)S(1)} %bitcast.92, bf16[384,4,64]{0,2,1:T(8,128)(2,1)} %get-tuple-element.177), kind=kOutput, calls=%fused_computation.33 | convolution fusion | flops 81984000 | bytes 5271552 | tf_op jit(solution)/shard_map/while/body/eval_jaxpr/cond/branch_1_fun/qhd,khd->hqk/dot_general | solution.py:63
  56.0 14.0 %fusion.2 = f32[4,384,3,128]{1,2,3,0:T(4,128)S(1)} fusion(f32[4,384,3,128]{1,3,2,0:T(8,128)S(1)} %bitcast.88), kind=kOutput, calls=%fused_computation.5 | output fusion | flops 74907648 | bytes 4718592 | tf_op jit(solution)/shard_map/reduce-window
  70.1 0.5 broadcast_add_fusion
  70.6 0.2 copy.79
  70.9 1.5 copy-done
  72.3 3.6 fusion.8
  76.0 0.3 fusion.27
  76.3 0.8 constant_dynamic-update-slice_fusion
  77.1 0.6 bitcast_dynamic-update-slice_fusion
  78.0 0.8 reduce_sum.74
  78.7 0.8 fusion.24
  79.5 1.6 fusion.22
  81.1 0.2 copy.84
  81.3 0.1 copy.85
  81.5 0.5 mul.104
  81.9 0.5 mul.105
  82.5 0.7 multiply_convert_fusion.2
  83.2 4.8 %all-to-all-start = ((bf16[8,48,256]{2,1,0:T(8,128)(2,1)}), bf16[8,48,256]{2,1,0:T(8,128)(2,1)S(1)}, u32[]{:S(2)}, u32[]{:S(2)}) async-start(bf16[8,48,256]{2,1,0:T(8,128)(2,1)} %multiply_convert_fusion.2), calls=%async_computation | async-start | bytes 393216 | tf_op jit(solution)/shard_map/all_to_all | solution.py:126
  88.5 0.2 select_reduce_fusion.1
  89.5 6.8 %all-to-all-done = bf16[8,48,256]{2,1,0:T(8,128)(2,1)S(1)} async-done(((bf16[8,48,256]{2,1,0:T(8,128)(2,1)}), bf16[8,48,256]{2,1,0:T(8,128)(2,1)S(1)}, u32[]{:S(2)}, u32[]{:S(2)}) %all-to-all-start) | async-done | bytes 196640 | tf_op jit(solution)/shard_map/all_to_all | solution.py:126
  96.4 5.1 %multiply_reduce_fusion.1 = (f32[48]{0:T(128)S(1)}, f32[48,2048]{1,0:T(8,128)S(1)}) fusion(bf16[48,2048]{1,0:T(8,128)(2,1)S(1)} %bitcast.94, bf16[2048,2048]{1,0:T(8,128)(2,1)} %all-gather.3.cloned.1.call-done, bf16[48,2048]{1,0:T(8,128)(2,1)S(1)} %copy-done.1), kind=kOutput, calls=%fused_computation.54 | convolution fusion | flops 403242944 | bytes 9175232 | tf_op jit(solution)/shard_map/dot_general | solution.py:127
  101.6 1.1 gather_fusion
  102.9 96.4 %all_to_all.26 = bf16[4,1,48,2048]{3,2,1,0:T(8,128)(2,1)} all-to-all(bf16[4,1,48,2048]{3,2,1,0:T(8,128)(2,1)S(1)} %broadcast_select_fusion), channel_id=1, replica_groups=mesh['sp'=4,'tp'=8] {'sp'}, dimensions={0} | all-to-all | bytes 1572864 | tf_op jit(solution)/shard_map/all_to_all | solution.py:140
  199.4 63.5 %all-gather.5.cloned.1.call-done = bf16[32,1,48,2048]{3,2,1,0:T(8,128)(2,1)} async-done(((bf16[4,1,48,2048]{3,2,1,0:T(8,128)(2,1)}), bf16[32,1,48,2048]{3,2,1,0:T(8,128)(2,1)}) %all-gather.5.cloned.1.call-update) | async-done | bytes 6291472 | tf_op jit(solution)/shard_map/all_gather | solution.py:147
  262.9 10.0 %fusion.18 = f32[1536,896]{1,0:T(8,128)S(1)} fusion(bf16[1536,2048]{1,0:T(8,128)(2,1)} %bitcast.101, bf16[1,2048,896]{2,1,0:T(8,128)(2,1)} %param.25), kind=kOutput, calls=%fused_computation.38 | convolution fusion | flops 5637144576 | bytes 15466496 | tf_op jit(solution)/shard_map/dot_general | solution.py:14
  272.9 7.1 %multiply_convert_fusion = bf16[1536,896]{1,0:T(8,128)(2,1)S(1)} fusion(f32[1536,896]{1,0:T(8,128)S(1)} %fusion.18, bf16[1536,2048]{1,0:T(8,128)(2,1)S(1)} %bitcast.102, bf16[1,2048,896]{2,1,0:T(8,128)(2,1)S(1)} %copy-done.7), kind=kOutput, calls=%fused_computation.35 | convolution fusion | flops 5645402112 | bytes 18219008 | tf_op jit(solution)/shard_map/dot_general | solution.py:15
  280.0 8.7 %convert_bitcast_fusion.1 = bf16[32,1,48,2048]{3,2,0,1:T(8,128)(2,1)} fusion(bf16[32,48,896]{2,1,0:T(8,128)(2,1)S(1)} %bitcast.103, bf16[1,896,2048]{2,1,0:T(8,128)(2,1)S(1)} %copy-done.8), kind=kOutput, calls=%fused_computation.34 | convolution fusion | flops 5640290304 | bytes 12713984 | tf_op jit(solution)/shard_map/dot_general | solution.py:17
  288.8 68.5 %reduce-scatter.2.cloned.1.call-done = bf16[4,1,48,2048]{3,2,0,1:T(8,128)(2,1)} async-done(((bf16[32,1,48,2048]{3,2,0,1:T(8,128)(2,1)}), bf16[4,1,48,2048]{3,2,0,1:T(8,128)(2,1)}) %reduce-scatter.2.cloned.1.call-update) | async-done | bytes 786448 | tf_op jit(solution)/shard_map/reduce_scatter | solution.py:157
  357.3 3.7 all-to-all-start.2
  361.5 8.6 %all-to-all-done.2 = bf16[4,1,48,2048]{3,2,1,0:T(8,128)(2,1)S(1)} async-done(((bf16[4,1,48,2048]{3,2,1,0:T(8,128)(2,1)}), bf16[4,1,48,2048]{3,2,1,0:T(8,128)(2,1)S(1)}, u32[]{:S(2)}, u32[]{:S(2)}) %all-to-all-start.2) | async-done | bytes 786464 | tf_op jit(solution)/shard_map/all_to_all | solution.py:158
  370.1 0.8 gather_fusion.1
  370.9 0.3 reshape.183
  371.2 2.1 multiply_reduce_fusion
  373.3 0.7 add_convert_fusion
  (64 shorter events, 2.3 us)
Async XLA Ops:
  6.5 89.9 %all-gather.3.cloned.1.call-start = ((), (), s32[]{:S(2)}) async-start(), calls=%async_computation.4 | async-start | bytes 9437184 | tf_op jit(solution)/shard_map/all_gather | solution.py:129
  70.6 1.7 copy-start
  79.5 2.9 copy-start.4
  81.1 7.0 %copy-start.3 = (s32[48,2]{0,1:T(2,128)S(1)}, s32[48,2]{0,1:T(2,128)}, u32[]{:S(2)}) copy-start(s32[48,2]{0,1:T(2,128)} %param.28) | copy-start | bytes 1156
  81.3 15.1 %copy-start.1 = (bf16[48,2048]{1,0:T(8,128)(2,1)S(1)}, bf16[48,2048]{1,0:T(8,128)(2,1)}, u32[]{:S(2)}) copy-start(bf16[48,2048]{1,0:T(8,128)(2,1)} %param.23) | copy-start | bytes 589828
  83.2 13.1 %all-to-all-start = ((bf16[8,48,256]{2,1,0:T(8,128)(2,1)}), bf16[8,48,256]{2,1,0:T(8,128)(2,1)S(1)}, u32[]{:S(2)}, u32[]{:S(2)}) async-start(bf16[8,48,256]{2,1,0:T(8,128)(2,1)} %multiply_convert_fusion.2), calls=%async_computation | async-start | bytes 393216 | tf_op jit(solution)/shard_map/all_to_all | solution.py:126
  88.0 174.9 %all-gather.5.cloned.1.call-start = ((), (), s32[]{:S(2)}) async-start(), calls=%async_computation.5 | async-start | bytes 7077888 | tf_op jit(solution)/shard_map/all_gather | solution.py:147
  96.4 5.1 %copy-start.2 = (f32[2048]{0:T(1024)S(1)}, f32[2048]{0:T(1024)}, u32[]{:S(2)}) copy-start(f32[2048]{0:T(1024)} %param.24) | copy-start | bytes 24580
  199.3 158.0 %reduce-scatter.2.cloned.1.call-start = ((), (), s32[]{:S(2)}) async-start(), calls=%async_computation.6 | async-start | bytes 7077888 | tf_op jit(solution)/shard_map/reduce_scatter | solution.py:157
  262.9 10.0 %copy-start.6 = (bf16[32,1,48,2048]{3,2,1,0:T(8,128)(2,1)S(1)}, bf16[32,1,48,2048]{3,2,1,0:T(8,128)(2,1)}, u32[]{:S(2)}) copy-start(bf16[32,1,48,2048]{3,2,1,0:T(8,128)(2,1)} %all-gather.5.cloned.1.call-done) | copy-start | bytes 18874372
  262.9 10.0 %copy-start.7 = (bf16[1,2048,896]{2,1,0:T(8,128)(2,1)S(1)}, bf16[1,2048,896]{2,1,0:T(8,128)(2,1)}, u32[]{:S(2)}) copy-start(bf16[1,2048,896]{2,1,0:T(8,128)(2,1)} %param.26) | copy-start | bytes 11010052
  272.9 7.1 %copy-start.8 = (bf16[1,896,2048]{2,1,0:T(8,128)(2,1)S(1)}, bf16[1,896,2048]{2,1,0:T(8,128)(2,1)}, u32[]{:S(2)}) copy-start(bf16[1,896,2048]{2,1,0:T(8,128)(2,1)} %param.27) | copy-start | bytes 11010052
  288.8 72.6 %copy-start.5 = (f32[48,2]{0,1:T(2,128)S(1)}, f32[48,2]{0,1:T(2,128)}, u32[]{:S(2)}) copy-start(f32[48,2]{0,1:T(2,128)} %param.29) | copy-start | bytes 1156
  357.3 12.7 %all-to-all-start.2 = ((bf16[4,1,48,2048]{3,2,1,0:T(8,128)(2,1)}), bf16[4,1,48,2048]{3,2,1,0:T(8,128)(2,1)S(1)}, u32[]{:S(2)}, u32[]{:S(2)}) async-start(bf16[4,1,48,2048]{3,2,1,0:T(8,128)(2,1)} %bitcast.96), calls=%async_computation.3 | async-start | bytes 1572864 | tf_op jit(solution)/shard_map/all_to_all | solution.py:158
Sparse Core Ops, SparseCore 0:
  8.9 84.8 all-gather.2
  199.4 63.4 all-gather.4
  288.9 68.3 reduce-scatter.1
where the time goes:
time: 382 us; the launch traced here: 380 us
  waiting for transfers between devices  148 us (39%)
  blocking collectives  133 us (35%)
  matrix products  35.5 us (9%)
  other arithmetic  26.7 us (7%)
  local copies, waits for them, and re-layouts  14.7 us (4%)
  between operations  13.4 us (4%)
  starting transfers between devices  8.62 us (2%)
    all_to_all x1, blocking collectives, on_device(): lax.all_to_all(outgoing.reshape(seq_devices, local_experts, capacity, mod...  96.4 us
    reduce_scatter x1, waiting for transfers between devices, on_device(): lax.psum_scatter(partials.astype(jnp.bfloat16), 'tp', scatter_dimension=0...  68.5 us
    all_gather x1, waiting for transfers between devices, on_device(): row_piece = lax.all_gather(arrived, 'tp', axis=0, tiled=True)  63.5 us
    another operation x2, other arithmetic  14.1 us
    all_gather x1, blocking collectives, on_device(): key_piece = lax.all_gather(keys, 'sp', axis=0, tiled=True)  13.4 us
    all_gather x1, blocking collectives, on_device(): value_piece = lax.all_gather(values, 'sp', axis=0, tiled=True)  12.4 us
    all_gather x1, blocking collectives, on_device(): bias_piece = lax.all_gather(key_bias, 'sp', axis=0, tiled=True)  11 us
    dot_general x1, matrix products, expert_partial(): jnp.dot(row_block, gate_matrix, preferred_element_type=jnp.float32)  9.96 us
  transfers between devices with their start and end apart: 5, of which 4 were waited for; matrix products, arithmetic and copies ran while one was open for 10% of the time, Pallas kernels for 0%

commit v1 on v0

--- a/solution.py
+++ b/solution.py
@@ -4,6 +4,17 @@
 from jax.sharding import PartitionSpec as P
 
 epsilon = 1e-06
+
+
+def ring_gather(x, axis, dim):
+    ways = lax.axis_size(axis)
+    pieces = [x]
+    for far in range(1, ways):
+        pieces.append(
+            lax.ppermute(pieces[far - 1], axis, [(d, (d - 1) % ways) for d in range(ways)])
+        )
+    line = jnp.concatenate(pieces, axis=dim)
+    return jnp.roll(line, lax.axis_index(axis) * x.shape[dim], axis=dim)
 
 
 def rms_scaled(values_in):
@@ -144,7 +155,7 @@
         concat_axis=0,
         tiled=True,
     )
-    row_piece = lax.all_gather(arrived, "tp", axis=0, tiled=True)
+    row_piece = ring_gather(arrived, "tp", 0)
     count_rows = row_piece.shape[0]
     partials = jnp.stack(
         [

time: 382 us -> 431 us (1.13)
  local copies, waits for them, and re-layouts: 14.7 us -> 39.4 us
  starting transfers between devices: 8.62 us -> 31.4 us
  loops' own time: 0.31 us -> 8.55 us
    all_gather x1 -> x0, waiting for transfers between devices: 63.5 us -> none  [on_device(): row_piece = lax.all_gather(arrived, 'tp', axis=0, tiled=True)]
    ppermute x0 -> x7, waiting for transfers between devices: none -> 58.3 us  [ring_gather(): lax.ppermute(pieces[far - 1], axis, [(d, (d - 1) % ways) for d in range(w...]
    ppermute x0 -> x7, starting transfers between devices: none -> 22.9 us  [ring_gather(): lax.ppermute(pieces[far - 1], axis, [(d, (d - 1) % ways) for d in range(w...]
    unnamed x21 -> x40, local copies, waits for them, and re-layouts: 4.15 us -> 24.4 us
    another operation x1, loops' own time: 0.2 us -> 8.44 us  [on_device(): lax.fori_loop(0, key_piece.shape[0] // rows_own, visit, empty_state)]
  transfers between devices with their start and end apart: 5 -> 11, of which waited for: 4 -> 10; matrix products, arithmetic and copies ran while one was open for 10% -> 11% of each run, Pallas kernels for 0% -> 0%
where the time goes in v1:
time: 431 us; the launch traced here: 430 us
  waiting for transfers between devices  145 us (34%)
  blocking collectives  133 us (31%)
  local copies, waits for them, and re-layouts  39.4 us (9%)
  matrix products  32.4 us (8%)
  starting transfers between devices  31.4 us (7%)
  other arithmetic  26.7 us (6%)
  between operations  14 us (3%)
  loops' own time  8.55 us (2%)
    all_to_all x1, blocking collectives, on_device(): lax.all_to_all(outgoing.reshape(seq_devices, local_experts, capacity, mod...  96.2 us
    reduce_scatter x1, waiting for transfers between devices, on_device(): lax.psum_scatter(partials.astype(jnp.bfloat16), 'tp', scatter_dimension=0...  70.2 us
    ppermute x7, waiting for transfers between devices, ring_gather(): lax.ppermute(pieces[far - 1], axis, [(d, (d - 1) % ways) for d in range(w...  58.3 us
    unnamed x40, local copies, waits for them, and re-layouts  24.4 us
    ppermute x7, starting transfers between devices, ring_gather(): lax.ppermute(pieces[far - 1], axis, [(d, (d - 1) % ways) for d in range(w...  22.9 us
    another operation x2, other arithmetic  14.1 us
    all_gather x1, blocking collectives, on_device(): key_piece = lax.all_gather(keys, 'sp', axis=0, tiled=True)  13.4 us
    all_gather x1, blocking collectives, on_device(): value_piece = lax.all_gather(values, 'sp', axis=0, tiled=True)  12.4 us
  transfers between devices with their start and end apart: 11, of which 10 were waited for; matrix products, arithmetic and copies ran while one was open for 11% of the time, Pallas kernels for 0%

profile of v1, /device:TPU:0, one launch (start us, length us, event | category | flops | bytes accessed | tf_op | source)
XLA Modules:
  0.0 430.1 jit_solution(11437114893456932746)
XLA Ops:
  7.3 1.1 copy.81
  8.4 1.1 copy.82
  9.4 1.7 copy.83
  11.2 11.0 %all_gather.14 = bf16[1536,4]{0,1:T(4,128)(2,1)} all-gather(bf16[384,4]{0,1:T(4,128)(2,1)} %param.20), channel_id=1, replica_groups=mesh['sp'=4,'tp'=8] {'sp'}, dimensions={0}, use_global_device_ids=true | all-gather | bytes 15360 | tf_op jit(solution)/shard_map/all_gather | solution.py:103
  22.2 12.4 %all_gather.12 = bf16[1536,256]{0,1:T(8,128)(2,1)} all-gather(bf16[384,256]{0,1:T(8,128)(2,1)S(1)} %copy.81), channel_id=1, replica_groups=mesh['sp'=4,'tp'=8] {'sp'}, dimensions={0}, use_global_device_ids=true | all-gather | bytes 983040 | tf_op jit(solution)/shard_map/all_gather | solution.py:102
  34.5 13.4 %all_gather.13 = bf16[1536,256]{0,1:T(8,128)(2,1)} all-gather(bf16[384,256]{0,1:T(8,128)(2,1)S(1)} %copy.82), channel_id=1, replica_groups=mesh['sp'=4,'tp'=8] {'sp'}, dimensions={0}, use_global_device_ids=true | all-gather | bytes 983040 | tf_op jit(solution)/shard_map/all_gather | solution.py:101
  47.9 1.3 broadcast_in_dim.84
  49.8 36.4 %while.17 = (s32[]{:T(128)}, f32[4,384,256]{1,2,0:T(8,128)}, f32[4,4,384]{2,1,0:T(4,128)}, s32[]{:T(128)}, bf16[1536,256]{0,1:T(8,128)(2,1)}, /*index=5*/bf16[15...) while((s32[]{:T(128)}, f32[4,384,256]{1,2,0:T(8,128)}, ...), condition=%wide.region_6.7_spmd.clone.clone, body=%wide.region_0.6_spmd.clone.clone.sunk | while | flops 246117120 | bytes 38572464 | solution.py:125
  49.8 28.0 %conditional.4 = ((f32[4,384,256]{1,2,0:T(8,128)}, f32[4,4,384]{2,1,0:T(4,128)})) conditional(s32[]{:T(128)} %convert_element_type.76, (f32[4,384,256]{1,2,0:T(8,128)}, f32[4,4,384]{2,1,0:T(4,128)}) %tuple.53, (s32[]{:T(128)}, bf16[1536,256]{0,1:T(8,128)(2,1)}, s32[]{:T(128)}, bf16[1536,256]{0,1:T(8,128)(2,1)}, bf16[384,4,64]{0,2,1:T(8,128)(2,1)}, ...), branch_computations={%region_1.0_spmd, %region_2.5_spmd} | conditional | flops 246117120 | bytes 38570716 | solution.py:123
  49.8 1.1 constant_dynamic-slice_fusion
  51.7 4.3 fusion.15
  56.0 14.0 %fusion.2 = f32[4,384,3,128]{1,2,3,0:T(4,128)S(1)} fusion(f32[4,384,3,128]{1,3,2,0:T(8,128)S(1)} %bitcast.90), kind=kOutput, calls=%fused_computation.5 | output fusion | flops 74907648 | bytes 4718592 | tf_op jit(solution)/shard_map/reduce-window
  70.9 1.5 copy-done
  72.3 3.6 fusion.8
  87.8 1.7 fusion.25
  91.6 4.8 %all-to-all-start = ((bf16[8,48,256]{2,1,0:T(8,128)(2,1)}), bf16[8,48,256]{2,1,0:T(8,128)(2,1)S(1)}, u32[]{:S(2)}, u32[]{:S(2)}) async-start(bf16[8,48,256]{2,1,0:T(8,128)(2,1)} %multiply_convert_fusion.2), calls=%async_computation | async-start | bytes 393216 | tf_op jit(solution)/shard_map/all_to_all | solution.py:137
  97.8 6.8 %all-to-all-done = bf16[8,48,256]{2,1,0:T(8,128)(2,1)S(1)} async-done(((bf16[8,48,256]{2,1,0:T(8,128)(2,1)}), bf16[8,48,256]{2,1,0:T(8,128)(2,1)S(1)}, u32[]{:S(2)}, u32[]{:S(2)}) %all-to-all-start) | async-done | bytes 196640 | tf_op jit(solution)/shard_map/all_to_all | solution.py:137
  104.7 5.1 %multiply_reduce_fusion.1 = (f32[48]{0:T(128)S(1)}, f32[48,2048]{1,0:T(8,128)S(1)}) fusion(bf16[48,2048]{1,0:T(8,128)(2,1)S(1)} %bitcast.98, bf16[2048,2048]{1,0:T(8,128)(2,1)} %all-gather.2.cloned.1.call-done, bf16[48,2048]{1,0:T(8,128)(2,1)S(1)} %copy-done.3), kind=kOutput, calls=%fused_computation.55 | convolution fusion | flops 403242944 | bytes 9175232 | tf_op jit(solution)/shard_map/dot_general | solution.py:138
  109.9 1.1 gather_fusion
  111.2 96.2 %all_to_all.26 = bf16[4,1,48,2048]{3,2,1,0:T(8,128)(2,1)S(1)} all-to-all(bf16[4,1,48,2048]{3,2,1,0:T(8,128)(2,1)S(1)} %broadcast_select_fusion), channel_id=1, replica_groups=mesh['sp'=4,'tp'=8] {'sp'}, dimensions={0} | all-to-all | bytes 1572864 | tf_op jit(solution)/shard_map/all_to_all | solution.py:151
  208.0 9.5 %collective-permute-done = bf16[4,1,48,2048]{3,2,1,0:T(8,128)(2,1)S(1)} collective-permute-done((bf16[4,1,48,2048]{3,2,1,0:T(8,128)(2,1)S(1)}, bf16[4,1,48,2048]{3,2,1,0:T(8,128)(2,1)S(1)}, u32[]{:S(2)}, u32[]{:S(2)}) %collective-permute-start) | collective-permute-done | bytes 786464 | tf_op jit(solution)/shard_map/ppermute | solution.py:14
  217.5 3.7 collective-permute-start.1
  221.2 9.5 %collective-permute-done.1 = bf16[4,1,48,2048]{3,2,1,0:T(8,128)(2,1)S(1)} collective-permute-done((bf16[4,1,48,2048]{3,2,1,0:T(8,128)(2,1)S(1)}, bf16[4,1,48,2048]{3,2,1,0:T(8,128)(2,1)S(1)}, u32[]{:S(2)}, u32[]{:S(2)}) %collective-permute-start.1) | collective-permute-done | bytes 786464 | tf_op jit(solution)/shard_map/ppermute | solution.py:14
  230.7 3.7 collective-permute-start.2
  234.4 9.5 %collective-permute-done.2 = bf16[4,1,48,2048]{3,2,1,0:T(8,128)(2,1)S(1)} collective-permute-done((bf16[4,1,48,2048]{3,2,1,0:T(8,128)(2,1)S(1)}, bf16[4,1,48,2048]{3,2,1,0:T(8,128)(2,1)S(1)}, u32[]{:S(2)}, u32[]{:S(2)}) %collective-permute-start.2) | collective-permute-done | bytes 786464 | tf_op jit(solution)/shard_map/ppermute | solution.py:14
  244.0 3.7 collective-permute-start.3
  247.7 9.5 %collective-permute-done.3 = bf16[4,1,48,2048]{3,2,1,0:T(8,128)(2,1)S(1)} collective-permute-done((bf16[4,1,48,2048]{3,2,1,0:T(8,128)(2,1)S(1)}, bf16[4,1,48,2048]{3,2,1,0:T(8,128)(2,1)S(1)}, u32[]{:S(2)}, u32[]{:S(2)}) %collective-permute-start.3) | collective-permute-done | bytes 786464 | tf_op jit(solution)/shard_map/ppermute | solution.py:14
  258.0 3.7 collective-permute-start.4
  261.7 9.5 %collective-permute-done.4 = bf16[4,1,48,2048]{3,2,1,0:T(8,128)(2,1)} collective-permute-done((bf16[4,1,48,2048]{3,2,1,0:T(8,128)(2,1)S(1)}, bf16[4,1,48,2048]{3,2,1,0:T(8,128)(2,1)}, u32[]{:S(2)}, u32[]{:S(2)}) %collective-permute-start.4) | collective-permute-done | bytes 786464 | tf_op jit(solution)/shard_map/ppermute | solution.py:14
  271.3 3.8 collective-permute-start.5
  277.9 7.0 %collective-permute-done.5 = bf16[4,1,48,2048]{3,2,1,0:T(8,128)(2,1)} collective-permute-done((bf16[4,1,48,2048]{3,2,1,0:T(8,128)(2,1)}, bf16[4,1,48,2048]{3,2,1,0:T(8,128)(2,1)}, u32[]{:S(2)}, u32[]{:S(2)}) %collective-permute-start.5) | collective-permute-done | bytes 786464 | tf_op jit(solution)/shard_map/ppermute | solution.py:14
  284.9 3.7 collective-permute-start.6
  290.5 2.1 constant_dynamic-update-slice_fusion.11
  292.6 2.1 constant_dynamic-update-slice_fusion.10
  294.7 3.7 collective-permute-done.6
  298.4 1.0 constant_dynamic-update-slice_fusion.9
  301.3 1.0 constant_dynamic-update-slice_fusion.6
  302.3 1.0 constant_dynamic-update-slice_fusion.5
  304.3 2.1 constant_dynamic-update-slice_fusion.3
  306.4 2.1 constant_dynamic-update-slice_fusion.2
  309.5 3.5 constant_dynamic-slice_fusion.2
  313.3 6.7 %fusion.21 = f32[1536,896]{1,0:T(8,128)S(1)} fusion(bf16[1536,2048]{1,0:T(8,128)(2,1)S(1)} %bitcast.94, bf16[1,2048,896]{2,1,0:T(8,128)(2,1)S(1)} %copy-done.8), kind=kOutput, calls=%fused_computation.39 | convolution fusion | flops 5637144576 | bytes 15466496 | tf_op jit(solution)/shard_map/dot_general | solution.py:25
  320.1 7.3 %multiply_convert_fusion = bf16[1536,896]{1,0:T(8,128)(2,1)S(1)} fusion(f32[1536,896]{1,0:T(8,128)S(1)} %fusion.21, bf16[1536,2048]{1,0:T(8,128)(2,1)S(1)} %bitcast.95, bf16[1,2048,896]{2,1,0:T(8,128)(2,1)S(1)} %copy-done.9), kind=kOutput, calls=%fused_computation.35 | convolution fusion | flops 5645402112 | bytes 18219008 | tf_op jit(solution)/shard_map/dot_general | solution.py:26
  327.4 8.7 %convert_bitcast_fusion.1 = bf16[32,1,48,2048]{3,2,0,1:T(8,128)(2,1)} fusion(bf16[32,48,896]{2,1,0:T(8,128)(2,1)S(1)} %bitcast.105, bf16[1,896,2048]{2,1,0:T(8,128)(2,1)S(1)} %copy-done.10), kind=kOutput, calls=%fused_computation.34 | convolution fusion | flops 5640290304 | bytes 12713984 | tf_op jit(solution)/shard_map/dot_general | solution.py:28
  336.1 70.2 %reduce-scatter.2.cloned.1.call-done = bf16[4,1,48,2048]{3,2,0,1:T(8,128)(2,1)} async-done(((bf16[32,1,48,2048]{3,2,0,1:T(8,128)(2,1)}), bf16[4,1,48,2048]{3,2,0,1:T(8,128)(2,1)}) %reduce-scatter.2.cloned.1.call-update) | async-done | bytes 786448 | tf_op jit(solution)/shard_map/reduce_scatter | solution.py:168
  406.3 3.6 all-to-all-start.2
  410.4 8.6 %all-to-all-done.2 = bf16[4,1,48,2048]{3,2,1,0:T(8,128)(2,1)S(1)} async-done(((bf16[4,1,48,2048]{3,2,1,0:T(8,128)(2,1)}), bf16[4,1,48,2048]{3,2,1,0:T(8,128)(2,1)S(1)}, u32[]{:S(2)}, u32[]{:S(2)}) %all-to-all-start.2) | async-done | bytes 786464 | tf_op jit(solution)/shard_map/all_to_all | solution.py:169
  420.1 2.0 multiply_reduce_fusion
  (96 shorter events, 22.7 us)
Async XLA Ops:
  6.5 98.1 %all-gather.2.cloned.1.call-start = ((), (), s32[]{:S(2)}) async-start(), calls=%async_computation.4 | async-start | bytes 9437184 | tf_op jit(solution)/shard_map/all_gather | solution.py:140
  70.6 1.7 copy-start
  86.2 4.5 %copy-start.6 = (f32[4,64]{1,0:T(4,128)S(1)}, f32[4,64]{1,0:T(4,128)}, u32[]{:S(2)}) copy-start(f32[4,64]{1,0:T(4,128)} %param.21) | copy-start | bytes 3076
  86.2 10.2 %copy-start.5 = (s32[48,2]{0,1:T(2,128)S(1)}, s32[48,2]{0,1:T(2,128)}, u32[]{:S(2)}) copy-start(s32[48,2]{0,1:T(2,128)} %param.28) | copy-start | bytes 1156
  87.7 16.9 %copy-start.3 = (bf16[48,2048]{1,0:T(8,128)(2,1)S(1)}, bf16[48,2048]{1,0:T(8,128)(2,1)}, u32[]{:S(2)}) copy-start(bf16[48,2048]{1,0:T(8,128)(2,1)} %param.23) | copy-start | bytes 589828
  91.6 13.1 %all-to-all-start = ((bf16[8,48,256]{2,1,0:T(8,128)(2,1)}), bf16[8,48,256]{2,1,0:T(8,128)(2,1)S(1)}, u32[]{:S(2)}, u32[]{:S(2)}) async-start(bf16[8,48,256]{2,1,0:T(8,128)(2,1)} %multiply_convert_fusion.2), calls=%async_computation | async-start | bytes 393216 | tf_op jit(solution)/shard_map/all_to_all | solution.py:137
  96.3 310.0 %reduce-scatter.2.cloned.1.call-start = ((), (), s32[]{:S(2)}) async-start(), calls=%async_computation.5 | async-start | bytes 7077888 | tf_op jit(solution)/shard_map/reduce_scatter | solution.py:168
  104.7 5.1 %copy-start.4 = (f32[2048]{0:T(1024)S(1)}, f32[2048]{0:T(1024)}, u32[]{:S(2)}) copy-start(f32[2048]{0:T(1024)} %param.24) | copy-start | bytes 24580
  207.4 10.1 %collective-permute-start = (bf16[4,1,48,2048]{3,2,1,0:T(8,128)(2,1)S(1)}, bf16[4,1,48,2048]{3,2,1,0:T(8,128)(2,1)S(1)}, u32[]{:S(2)}, u32[]{:S(2)}) collective-permute-start(bf16[4,1,48,2048]{3,2,1,0:T(8,128)(2,1)S(1)} %all_to_all.26), channel_id=1, source_target_pairs={{0,7},{1,0},{2,1},{3,2},{4,3},{5,4},{6,5},{7,6},{8,15},{9,8},{10,9... | collective-permute-start | bytes 2359304 | tf_op jit(solution)/shard_map/ppermute | solution.py:14
  217.5 13.2 %collective-permute-start.1 = (bf16[4,1,48,2048]{3,2,1,0:T(8,128)(2,1)S(1)}, bf16[4,1,48,2048]{3,2,1,0:T(8,128)(2,1)S(1)}, u32[]{:S(2)}, u32[]{:S(2)}) collective-permute-start(bf16[4,1,48,2048]{3,2,1,0:T(8,128)(2,1)S(1)} %collective-permute-done), channel_id=1, source_target_pairs={{0,7},{1,0},{2,1},{3,2},{4,3},{5,4},{6,5},{7,6},{8,15},{9,8},{10,9... | collective-permute-start | bytes 2359304 | tf_op jit(solution)/shard_map/ppermute | solution.py:14
  230.7 13.2 %collective-permute-start.2 = (bf16[4,1,48,2048]{3,2,1,0:T(8,128)(2,1)S(1)}, bf16[4,1,48,2048]{3,2,1,0:T(8,128)(2,1)S(1)}, u32[]{:S(2)}, u32[]{:S(2)}) collective-permute-start(bf16[4,1,48,2048]{3,2,1,0:T(8,128)(2,1)S(1)} %collective-permute-done.1), channel_id=1, source_target_pairs={{0,7},{1,0},{2,1},{3,2},{4,3},{5,4},{6,5},{7,6},{8,15},{9,8},{10,9... | collective-permute-start | bytes 2359304 | tf_op jit(solution)/shard_map/ppermute | solution.py:14
  244.0 13.2 %collective-permute-start.3 = (bf16[4,1,48,2048]{3,2,1,0:T(8,128)(2,1)S(1)}, bf16[4,1,48,2048]{3,2,1,0:T(8,128)(2,1)S(1)}, u32[]{:S(2)}, u32[]{:S(2)}) collective-permute-start(bf16[4,1,48,2048]{3,2,1,0:T(8,128)(2,1)S(1)} %collective-permute-done.2), channel_id=1, source_target_pairs={{0,7},{1,0},{2,1},{3,2},{4,3},{5,4},{6,5},{7,6},{8,15},{9,8},{10,9... | collective-permute-start | bytes 2359304 | tf_op jit(solution)/shard_map/ppermute | solution.py:14
  257.2 0.9 copy-start.1
  258.0 13.2 %collective-permute-start.4 = (bf16[4,1,48,2048]{3,2,1,0:T(8,128)(2,1)S(1)}, bf16[4,1,48,2048]{3,2,1,0:T(8,128)(2,1)}, u32[]{:S(2)}, u32[]{:S(2)}) collective-permute-start(bf16[4,1,48,2048]{3,2,1,0:T(8,128)(2,1)S(1)} %collective-permute-done.3), channel_id=1, source_target_pairs={{0,7},{1,0},{2,1},{3,2},{4,3},{5,4},{6,5},{7,6},{8,15},{9,8},{10,9... | collective-permute-start | bytes 2359304 | tf_op jit(solution)/shard_map/ppermute | solution.py:14
  271.3 13.6 %collective-permute-start.5 = (bf16[4,1,48,2048]{3,2,1,0:T(8,128)(2,1)}, bf16[4,1,48,2048]{3,2,1,0:T(8,128)(2,1)}, u32[]{:S(2)}, u32[]{:S(2)}) collective-permute-start(bf16[4,1,48,2048]{3,2,1,0:T(8,128)(2,1)} %collective-permute-done.4), channel_id=1, source_target_pairs={{0,7},{1,0},{2,1},{3,2},{4,3},{5,4},{6,5},{7,6},{8,15},{9,8},{10,9... | collective-permute-start | bytes 2359304 | tf_op jit(solution)/shard_map/ppermute | solution.py:14
  275.1 14.5 %copy-start.2 = (bf16[4,1,48,2048]{3,2,1,0:T(8,128)(2,1)S(1)}, bf16[4,1,48,2048]{3,2,1,0:T(8,128)(2,1)}, u32[]{:S(2)}) copy-start(bf16[4,1,48,2048]{3,2,1,0:T(8,128)(2,1)} %copy-done.1) | copy-start | bytes 2359300
  284.9 13.5 %collective-permute-start.6 = (bf16[4,1,48,2048]{3,2,1,0:T(8,128)(2,1)}, bf16[4,1,48,2048]{3,2,1,0:T(8,128)(2,1)S(1)}, u32[]{:S(2)}, u32[]{:S(2)}) collective-permute-start(bf16[4,1,48,2048]{3,2,1,0:T(8,128)(2,1)} %collective-permute-done.5), channel_id=1, source_target_pairs={{0,7},{1,0},{2,1},{3,2},{4,3},{5,4},{6,5},{7,6},{8,15},{9,8},{10,9... | collective-permute-start | bytes 2359304 | tf_op jit(solution)/shard_map/ppermute | solution.py:14
  309.5 3.9 copy-start.8
  313.3 6.7 %copy-start.9 = (bf16[1,2048,896]{2,1,0:T(8,128)(2,1)S(1)}, bf16[1,2048,896]{2,1,0:T(8,128)(2,1)}, u32[]{:S(2)}) copy-start(bf16[1,2048,896]{2,1,0:T(8,128)(2,1)} %param.26) | copy-start | bytes 11010052
  320.1 7.3 %copy-start.10 = (bf16[1,896,2048]{2,1,0:T(8,128)(2,1)S(1)}, bf16[1,896,2048]{2,1,0:T(8,128)(2,1)}, u32[]{:S(2)}) copy-start(bf16[1,896,2048]{2,1,0:T(8,128)(2,1)} %param.27) | copy-start | bytes 11010052
  336.1 74.2 %copy-start.7 = (f32[48,2]{0,1:T(2,128)S(1)}, f32[48,2]{0,1:T(2,128)}, u32[]{:S(2)}) copy-start(f32[48,2]{0,1:T(2,128)} %param.29) | copy-start | bytes 1156
  406.3 12.7 %all-to-all-start.2 = ((bf16[4,1,48,2048]{3,2,1,0:T(8,128)(2,1)}), bf16[4,1,48,2048]{3,2,1,0:T(8,128)(2,1)S(1)}, u32[]{:S(2)}, u32[]{:S(2)}) async-start(bf16[4,1,48,2048]{3,2,1,0:T(8,128)(2,1)} %bitcast.100), calls=%async_computation.3 | async-start | bytes 1572864 | tf_op jit(solution)/shard_map/all_to_all | solution.py:169
Sparse Core Ops, SparseCore 0:
  8.9 84.7 all-gather.1
  336.2 70.0 reduce-scatter.1
